TPU v7x, 32 devices: a whole 2x2x4 slice. The times are simulated.
32 devices in a mesh: fs: 16 (over z, y, x), tp: 2 (over core).
Axes of the slice: x: 2, y: 2, z: 4, core: 2. Of those that a mesh axis runs over, the one named last changes fastest.
Arguments:
- saved_inputs: bfloat16 [12288, 2048], P('fs'), may hold values from -8 to 8
- input_cot: bfloat16 [12288, 2048], P('fs', 'tp'), may hold values from -0.0546875 to 0.0546875
- gate_cot: bfloat16 [12288, 2048], P('fs', 'tp'), may hold values from -0.0546875 to 0.0546875
- input_master: float32 [2048, 2048], P('fs', 'tp'), may hold values from -6 to 6
- gate_master: float32 [2048, 2048], P('fs', 'tp'), may hold values from -6 to 6
- input_factor: bfloat16 [2048, 256], P('fs'), may hold values from -2 to 2
- gate_factor: bfloat16 [2048, 256], P('fs'), may hold values from -2 to 2
- input_first: float32 [256, 2048], P('fs', 'tp'), may hold values from -6 to 6
- input_second: float32 [256, 2048], P('fs', 'tp'), may hold values from 0.2 to 17
- gate_first: float32 [256, 2048], P('fs', 'tp'), may hold values from -6 to 6
- gate_second: float32 [256, 2048], P('fs', 'tp'), may hold values from 0.2 to 17
Outputs:
- input_step: float32 [2048, 2048], P('fs', 'tp')
- gate_step: float32 [2048, 2048], P('fs', 'tp')
- input_first_new: float32 [256, 2048], P('fs', 'tp')
- input_second_new: float32 [256, 2048], P('fs', 'tp')
- gate_first_new: float32 [256, 2048], P('fs', 'tp')
- gate_second_new: float32 [256, 2048], P('fs', 'tp')
- input_copy: bfloat16 [2048, 2048], P(None, 'tp')
- gate_copy: bfloat16 [2048, 2048], P(None, 'tp')
All inputs are finite; a program needn't handle non-finite values.
Results may differ from a plain program's by a relative error of at most 0.0004.
Values may be sent and summed in bfloat16 or wider, within the bound.
A program may use at most 64 MiB of HBM per device.

v0:
```python
import jax
import jax.numpy as jnp
from jax import lax
from jax.sharding import PartitionSpec as P

D = 2048
W = 2048
first_decay = 0.9
second_decay = 0.9
ratio_floor = 1e-08
mean_floor = 1e-06
step_size = 0.05


def moments(low_rank, first, second):
    first_new = first_decay * first + (1.0 - first_decay) * low_rank
    second_new = second_decay * second + (1.0 - second_decay) * low_rank * low_rank
    ratio = first_new / (jnp.sqrt(second_new) + ratio_floor)
    return (first_new, second_new, ratio)


def local(
    saved_inputs,
    input_cot,
    gate_cot,
    input_master,
    gate_master,
    input_factor,
    gate_factor,
    input_first,
    input_second,
    gate_first,
    gate_second,
):
    col_width = input_cot.shape[1]
    contract = (((0,), (0,)), ((), ()))
    factor_in = input_factor.astype(jnp.float32)
    factor_gate = gate_factor.astype(jnp.float32)
    whole_in, whole_gate = (
        lax.all_gather(input_factor, "fs", axis=0, tiled=True),
        lax.all_gather(gate_factor, "fs", axis=0, tiled=True),
    )
    partial_in = lax.dot_general(
        saved_inputs, input_cot, contract, preferred_element_type=jnp.float32
    )
    partial_gate = lax.dot_general(
        saved_inputs, gate_cot, contract, preferred_element_type=jnp.float32
    )
    cols_in = whole_in.astype(jnp.float32)
    cols_gate = whole_gate.astype(jnp.float32)
    term_in = lax.dot_general(cols_in, partial_in, contract, precision=lax.Precision.HIGHEST)
    term_gate = lax.dot_general(cols_gate, partial_gate, contract, precision=lax.Precision.HIGHEST)
    summed = lax.psum_scatter(
        jnp.concatenate([term_in, term_gate], axis=1), "fs", scatter_dimension=0, tiled=True
    )
    low_in = summed[:, :col_width]
    low_gate = summed[:, col_width:]
    first_in, second_in, ratio_in = moments(low_in, input_first, input_second)
    first_gate, second_gate, ratio_gate = moments(low_gate, gate_first, gate_second)
    piece_in = lax.all_gather(ratio_in, "fs", axis=0, tiled=True)
    piece_gate = lax.all_gather(ratio_gate, "fs", axis=0, tiled=True)
    cols_in = factor_in
    cols_gate = factor_gate
    dir_in = jnp.dot(cols_in, piece_in, precision=lax.Precision.HIGHEST)
    dir_gate = jnp.dot(cols_gate, piece_gate, precision=lax.Precision.HIGHEST)
    square_in, square_gate = lax.psum(
        (jnp.sum(dir_in * dir_in), jnp.sum(dir_gate * dir_gate)), ("fs", "tp")
    )
    step_in = dir_in * lax.rsqrt(square_in / (D * W) + mean_floor)
    step_gate = dir_gate * lax.rsqrt(square_gate / (D * W) + mean_floor)
    local_in = (input_master - step_size * step_in).astype(jnp.bfloat16)
    local_gate = (gate_master - step_size * step_gate).astype(jnp.bfloat16)
    copy_in, copy_gate = (
        lax.all_gather(local_in, "fs", axis=0, tiled=True),
        lax.all_gather(local_gate, "fs", axis=0, tiled=True),
    )
    return (step_in, step_gate, first_in, second_in, first_gate, second_gate, copy_in, copy_gate)


def solution(mesh):
    return jax.shard_map(
        local,
        mesh=mesh,
        in_specs=(
            P("fs", None),
            P("fs", "tp"),
            P("fs", "tp"),
            P("fs", "tp"),
            P("fs", "tp"),
            P("fs", None),
            P("fs", None),
            P("fs", "tp"),
            P("fs", "tp"),
            P("fs", "tp"),
            P("fs", "tp"),
        ),
        out_specs=(
            P("fs", "tp"),
            P("fs", "tp"),
            P("fs", "tp"),
            P("fs", "tp"),
            P("fs", "tp"),
            P("fs", "tp"),
            P(None, "tp"),
            P(None, "tp"),
        ),
        check_vma=False,
    )
```

profile of v0, /device:TPU:0, one launch (start us, length us, event | category | flops | bytes accessed | tf_op | source)
XLA Modules:
  0.0 569.3 jit_solution(10387800890137530023)
XLA Ops:
  7.2 0.0 copy-start
  7.2 0.0 all-gather.7.cloned.1.call-start
  7.2 0.7 all-gather.7.cloned.1.call-update
  7.9 0.0 all-gather.9.cloned.1.call-start
  8.0 0.7 all-gather.9.cloned.1.call-update
  8.7 0.0 reduce-scatter.4.cloned.1.call-start
  8.7 0.3 copy-done
  9.1 7.2 %fusion.4 = f32[2048,1024]{1,0:T(8,128)} fusion(bf16[768,2048]{1,0:T(8,128)(2,1)S(1)} %copy-done, bf16[768,1024]{1,0:T(8,128)(2,1)} %param.12), kind=kOutput, calls=%fused_computation.17 | convolution fusion | flops 3221225472 | bytes 13107200 | tf_op jit(solution)/shard_map/dot_general | solution.py:43
  16.2 0.0 copy-done.8
  16.2 5.7 %fusion.5 = f32[2048,1024]{1,0:T(8,128)} fusion(bf16[768,2048]{1,0:T(8,128)(2,1)S(1)} %copy-done, bf16[768,1024]{1,0:T(8,128)(2,1)S(1)} %copy-done.8), kind=kOutput, calls=%fused_computation.18 | convolution fusion | flops 3221225472 | bytes 13107200 | tf_op jit(solution)/shard_map/dot_general | solution.py:46
  21.9 46.7 %all-gather.7.cloned.1.call-done = bf16[2048,256]{1,0:T(8,128)(2,1)} async-done(((bf16[128,256]{1,0:T(8,128)(2,1)}), bf16[2048,256]{1,0:T(8,128)(2,1)}) %all-gather.7.cloned.1.call-update) | async-done | bytes 1048592 | tf_op jit(solution)/shard_map/all_gather | solution.py:40
  68.6 11.2 %convolution_bitcast_fusion.1 = f32[256,1024]{0,1:T(8,128)} fusion(f32[2048,1024]{1,0:T(8,128)} %fusion.4, bf16[2048,256]{1,0:T(8,128)(2,1)} %all-gather.7.cloned.1.call-done), kind=kOutput, calls=%fused_computation.2 | convolution fusion | flops 6442450944 | bytes 10485760 | tf_op jit(solution)/shard_map/dot_general | solution.py:51
  79.8 45.5 %all-gather.9.cloned.1.call-done = bf16[2048,256]{1,0:T(8,128)(2,1)} async-done(((bf16[128,256]{1,0:T(8,128)(2,1)}), bf16[2048,256]{1,0:T(8,128)(2,1)}) %all-gather.9.cloned.1.call-update) | async-done | bytes 1048592 | tf_op jit(solution)/shard_map/all_gather | solution.py:41
  125.3 9.5 %convolution_bitcast_fusion = f32[256,1024]{0,1:T(8,128)S(1)} fusion(f32[2048,1024]{1,0:T(8,128)} %fusion.5, bf16[2048,256]{1,0:T(8,128)(2,1)} %all-gather.9.cloned.1.call-done), kind=kOutput, calls=%fused_computation.1 | convolution fusion | flops 6442450944 | bytes 10485760 | tf_op jit(solution)/shard_map/dot_general | solution.py:52
  134.8 0.0 copy-done.1
  134.8 1.5 pad_maximum_fusion
  136.2 0.0 copy-start.2
  136.3 2.9 copy.65
  139.2 0.0 reduce-scatter.4.cloned.1.call-update
  139.2 0.0 all-gather.13.cloned.1.call-start
  139.3 80.6 %reduce-scatter.4.cloned.1.call-done = f32[16,2048]{1,0:T(8,128)} async-done(((f32[256,2048]{1,0:T(8,128)}), f32[16,2048]{1,0:T(8,128)}) %reduce-scatter.4.cloned.1.call-update) | async-done | bytes 131088 | tf_op jit(solution)/shard_map/reduce_scatter | solution.py:53
  219.9 0.0 copy-done.4
  219.9 0.0 copy-done.5
  219.9 0.0 copy-done.6
  219.9 0.0 copy-done.7
  219.9 1.6 add_divide_fusion
  221.5 0.0 all-gather.13.cloned.1.call-update
  221.5 0.0 all-gather.11.cloned.1.call-start
  221.6 0.5 all-gather.11.cloned.1.call-update
  222.1 0.0 all-gather.15.cloned.1.call-start
  222.2 2.0 copy.59
  224.2 50.4 %all-gather.13.cloned.1.call-done = f32[256,1024]{1,0:T(8,128)} async-done(((f32[16,1024]{1,0:T(8,128)}), f32[256,1024]{1,0:T(8,128)}) %all-gather.13.cloned.1.call-update) | async-done | bytes 1048592 | tf_op jit(solution)/shard_map/all_gather | solution.py:61
  274.6 3.7 multiply_reduce_fusion
  278.3 53.4 %all-gather.11.cloned.1.call-done = f32[256,1024]{1,0:T(8,128)} async-done(((f32[16,1024]{1,0:T(8,128)}), f32[256,1024]{1,0:T(8,128)}) %all-gather.11.cloned.1.call-update) | async-done | bytes 1048592 | tf_op jit(solution)/shard_map/all_gather | solution.py:60
  331.7 3.6 multiply_reduce_fusion.1
  335.4 38.6 %all-reduce = (f32[]{:T(128)}, f32[]{:T(128)}) all-reduce(f32[]{:T(128)} %get-tuple-element.47, f32[]{:T(128)} %get-tuple-element.49), channel_id=1, replica_groups=mesh['fs'=16,'tp'=2] {'fs','tp'}, use_global_device_ids=true, to_apply=%region_2.0 | all-reduce | flops 2 | bytes 16 | tf_op jit(solution)/shard_map/psum | solution.py:66
  374.7 2.2 subtract_convert_fusion.1
  376.8 0.0 all-gather.15.cloned.1.call-update
  376.9 0.0 all-gather.17.cloned.1.call-start
  376.9 2.0 copy.60
  379.7 2.2 subtract_convert_fusion
  381.8 0.0 all-gather.17.cloned.1.call-update
  381.9 2.0 copy.61
  383.9 2.0 copy.62
  385.9 80.5 %all-gather.15.cloned.1.call-done = bf16[2048,1024]{0,1:T(8,128)(2,1)} async-done(((bf16[128,1024]{0,1:T(8,128)(2,1)}), bf16[2048,1024]{0,1:T(8,128)(2,1)}) %all-gather.15.cloned.1.call-update) | async-done | bytes 4194320 | tf_op jit(solution)/shard_map/all_gather | solution.py:74
  466.4 6.4 %copy.63 = bf16[2048,1024]{1,0:T(8,128)(2,1)} copy(bf16[2048,1024]{0,1:T(8,128)(2,1)} %all-gather.15.cloned.1.call-done) | data formatting | bytes 8388608
  472.8 83.2 %all-gather.17.cloned.1.call-done = bf16[2048,1024]{0,1:T(8,128)(2,1)} async-done(((bf16[128,1024]{0,1:T(8,128)(2,1)}), bf16[2048,1024]{0,1:T(8,128)(2,1)}) %all-gather.17.cloned.1.call-update) | async-done | bytes 4194320 | tf_op jit(solution)/shard_map/all_gather | solution.py:75
  556.0 6.4 %copy.64 = bf16[2048,1024]{1,0:T(8,128)(2,1)} copy(bf16[2048,1024]{0,1:T(8,128)(2,1)} %all-gather.17.cloned.1.call-done) | data formatting | bytes 8388608
  (9 shorter events, 0.0 us)
Async XLA Ops:
  7.2 1.9 copy-start
  7.2 61.4 %all-gather.7.cloned.1.call-start = ((), (), s32[]{:S(2)}) async-start(), calls=%async_computation.1 | async-start | bytes 1114112 | tf_op jit(solution)/shard_map/all_gather | solution.py:40
  7.9 117.4 %all-gather.9.cloned.1.call-start = ((), (), s32[]{:S(2)}) async-start(), calls=%async_computation.2 | async-start | bytes 1114112 | tf_op jit(solution)/shard_map/all_gather | solution.py:41
  8.7 211.2 %reduce-scatter.4.cloned.1.call-start = ((), (), s32[]{:S(2)}) async-start(), calls=%async_computation.7 | async-start | bytes 2228224 | tf_op jit(solution)/shard_map/reduce_scatter | solution.py:53
  9.1 7.2 %copy-start.8 = (bf16[768,1024]{1,0:T(8,128)(2,1)S(1)}, bf16[768,1024]{1,0:T(8,128)(2,1)}, u32[]{:S(2)}) copy-start(bf16[768,1024]{1,0:T(8,128)(2,1)} %param.13) | copy-start | bytes 4718596
  125.3 9.5 %copy-start.1 = (f32[256,1024]{0,1:T(8,128)S(1)}, f32[256,1024]{0,1:T(8,128)}, u32[]{:S(2)}) copy-start(f32[256,1024]{0,1:T(8,128)} %convolution_bitcast_fusion.1) | copy-start | bytes 3145732
  136.2 83.6 %copy-start.4 = (f32[16,1024]{1,0:T(8,128)S(1)}, f32[16,1024]{1,0:T(8,128)}, u32[]{:S(2)}) copy-start(f32[16,1024]{1,0:T(8,128)} %param.21) | copy-start | bytes 196612
  136.2 83.6 %copy-start.5 = (f32[16,1024]{1,0:T(8,128)S(1)}, f32[16,1024]{1,0:T(8,128)}, u32[]{:S(2)}) copy-start(f32[16,1024]{1,0:T(8,128)} %param.20) | copy-start | bytes 196612
  136.2 83.6 %copy-start.6 = (f32[16,1024]{1,0:T(8,128)S(1)}, f32[16,1024]{1,0:T(8,128)}, u32[]{:S(2)}) copy-start(f32[16,1024]{1,0:T(8,128)} %param.19) | copy-start | bytes 196612
  136.2 83.6 %copy-start.7 = (f32[16,1024]{1,0:T(8,128)S(1)}, f32[16,1024]{1,0:T(8,128)}, u32[]{:S(2)}) copy-start(f32[16,1024]{1,0:T(8,128)} %param.18) | copy-start | bytes 196612
  136.2 138.3 %copy-start.2 = (bf16[128,256]{1,0:T(8,128)(2,1)S(1)}, bf16[128,256]{1,0:T(8,128)(2,1)}, u32[]{:S(2)}) copy-start(bf16[128,256]{1,0:T(8,128)(2,1)} %param.17) | copy-start | bytes 196612
  139.2 192.5 %copy-start.3 = (bf16[128,256]{1,0:T(8,128)(2,1)S(1)}, bf16[128,256]{1,0:T(8,128)(2,1)}, u32[]{:S(2)}) copy-start(bf16[128,256]{1,0:T(8,128)(2,1)} %param.16) | copy-start | bytes 196612
  139.2 135.4 %all-gather.13.cloned.1.call-start = ((), (), s32[]{:S(2)}) async-start(), calls=%async_computation.4 | async-start | bytes 1114112 | tf_op jit(solution)/shard_map/all_gather | solution.py:61
  221.5 110.2 %all-gather.11.cloned.1.call-start = ((), (), s32[]{:S(2)}) async-start(), calls=%async_computation.3 | async-start | bytes 1114112 | tf_op jit(solution)/shard_map/all_gather | solution.py:60
  222.1 244.3 %all-gather.15.cloned.1.call-start = ((), (), s32[]{:S(2)}) async-start(), calls=%async_computation.5 | async-start | bytes 4456448 | tf_op jit(solution)/shard_map/all_gather | solution.py:74
  376.9 179.2 %all-gather.17.cloned.1.call-start = ((), (), s32[]{:S(2)}) async-start(), calls=%async_computation.6 | async-start | bytes 4456448 | tf_op jit(solution)/shard_map/all_gather | solution.py:75
Sparse Core Ops, SparseCore 0:
  10.7 57.7 all-gather.6
  71.3 53.9 all-gather.8
  139.3 80.4 reduce-scatter.3
  223.0 51.4 all-gather.12
  277.8 53.9 all-gather.10
  377.0 89.3 all-gather.14
  469.1 86.8 all-gather.16
where the time goes:
time: 570 us; the launch traced here: 569 us
  waiting for transfers between devices  442 us (78%)
  matrix products  40.9 us (7%)
  blocking collectives  38.6 us (7%)
  local copies, waits for them, and re-layouts  24.2 us (4%)
  between operations  15.6 us (3%)
  other arithmetic  7.42 us (1%)
    all_gather x1, waiting for transfers between devices, local(): lax.all_gather(local_gate, 'fs', axis=0, tiled=True)  83.2 us
    reduce_scatter x1, waiting for transfers between devices, local(): lax.psum_scatter(jnp.concatenate([term_in, term_gate], axis=1), 'fs', sca...  80.6 us
    all_gather x1, waiting for transfers between devices, local(): lax.all_gather(local_in, 'fs', axis=0, tiled=True)  80.5 us
    all_gather x1, waiting for transfers between devices, local(): piece_in = lax.all_gather(ratio_in, 'fs', axis=0, tiled=True)  53.4 us
    all_gather x1, waiting for transfers between devices, local(): piece_gate = lax.all_gather(ratio_gate, 'fs', axis=0, tiled=True)  50.4 us
    all_gather x1, waiting for transfers between devices, local(): lax.all_gather(input_factor, 'fs', axis=0, tiled=True)  46.7 us
    all_gather x1, waiting for transfers between devices, local(): lax.all_gather(gate_factor, 'fs', axis=0, tiled=True)  45.5 us
    psum x1, blocking collectives, local(): lax.psum((jnp.sum(dir_in * dir_in), jnp.sum(dir_gate * dir_gate)), ('fs',...  38.6 us
  transfers between devices with their start and end apart: 7, of which 7 were waited for; matrix products, arithmetic and copies ran while one was open for 8% of the time, Pallas kernels for 0%

commit v1 on v0

--- a/solution.py
+++ b/solution.py
@@ -10,6 +10,11 @@
 ratio_floor = 1e-08
 mean_floor = 1e-06
 step_size = 0.05
+
+
+def axis_by_axis(array, inner_axis, outer_axis):
+    half = lax.psum(array, inner_axis)
+    return lax.psum(half, outer_axis)
 
 
 def moments(low_rank, first, second):
@@ -63,8 +68,8 @@
     cols_gate = factor_gate
     dir_in = jnp.dot(cols_in, piece_in, precision=lax.Precision.HIGHEST)
     dir_gate = jnp.dot(cols_gate, piece_gate, precision=lax.Precision.HIGHEST)
-    square_in, square_gate = lax.psum(
-        (jnp.sum(dir_in * dir_in), jnp.sum(dir_gate * dir_gate)), ("fs", "tp")
+    square_in, square_gate = axis_by_axis(
+        (jnp.sum(dir_in * dir_in), jnp.sum(dir_gate * dir_gate)), "fs", "tp"
     )
     step_in = dir_in * lax.rsqrt(square_in / (D * W) + mean_floor)
     step_gate = dir_gate * lax.rsqrt(square_gate / (D * W) + mean_floor)

time: 570 us -> 570 us (level)
    psum x1 -> x2, blocking collectives: 38.6 us -> 43.4 us  [the longest x1 40.3 us: axis_by_axis(): half = lax.psum(array, inner_axis)]
where the time goes in v1:
time: 570 us; the launch traced here: 569 us
  waiting for transfers between devices  437 us (77%)
  blocking collectives  43.4 us (8%)
  matrix products  40.8 us (7%)
  local copies, waits for them, and re-layouts  24.3 us (4%)
  between operations  15.6 us (3%)
  other arithmetic  7.46 us (1%)
    all_gather x1, waiting for transfers between devices, local(): lax.all_gather(local_gate, 'fs', axis=0, tiled=True)  83.2 us
    reduce_scatter x1, waiting for transfers between devices, local(): lax.psum_scatter(jnp.concatenate([term_in, term_gate], axis=1), 'fs', sca...  80.4 us
    all_gather x1, waiting for transfers between devices, local(): lax.all_gather(local_in, 'fs', axis=0, tiled=True)  75.6 us
    all_gather x1, waiting for transfers between devices, local(): piece_in = lax.all_gather(ratio_in, 'fs', axis=0, tiled=True)  53.5 us
    all_gather x1, waiting for transfers between devices, local(): piece_gate = lax.all_gather(ratio_gate, 'fs', axis=0, tiled=True)  50.6 us
    all_gather x1, waiting for transfers between devices, local(): lax.all_gather(input_factor, 'fs', axis=0, tiled=True)  46.7 us
    all_gather x1, waiting for transfers between devices, local(): lax.all_gather(gate_factor, 'fs', axis=0, tiled=True)  45.5 us
    psum x1, blocking collectives, axis_by_axis(): half = lax.psum(array, inner_axis)  40.3 us
  transfers between devices with their start and end apart: 7, of which 7 were waited for; matrix products, arithmetic and copies ran while one was open for 8% of the time, Pallas kernels for 0%

profile of v1, /device:TPU:0, one launch (start us, length us, event | category | flops | bytes accessed | tf_op | source)
XLA Modules:
  0.0 569.4 jit_solution(12057421192152946405)
XLA Ops:
  7.2 0.0 copy-start
  7.2 0.0 all-gather.7.cloned.1.call-start
  7.2 0.7 all-gather.7.cloned.1.call-update
  7.9 0.0 all-gather.9.cloned.1.call-start
  8.0 0.7 all-gather.9.cloned.1.call-update
  8.7 0.0 reduce-scatter.4.cloned.1.call-start
  8.7 0.3 copy-done
  9.1 7.2 %fusion.4 = f32[2048,1024]{1,0:T(8,128)} fusion(bf16[768,2048]{1,0:T(8,128)(2,1)S(1)} %copy-done, bf16[768,1024]{1,0:T(8,128)(2,1)} %param.12), kind=kOutput, calls=%fused_computation.17 | convolution fusion | flops 3221225472 | bytes 13107200 | tf_op jit(solution)/shard_map/dot_general | solution.py:48
  16.2 0.0 copy-done.8
  16.2 5.7 %fusion.5 = f32[2048,1024]{1,0:T(8,128)} fusion(bf16[768,2048]{1,0:T(8,128)(2,1)S(1)} %copy-done, bf16[768,1024]{1,0:T(8,128)(2,1)S(1)} %copy-done.8), kind=kOutput, calls=%fused_computation.18 | convolution fusion | flops 3221225472 | bytes 13107200 | tf_op jit(solution)/shard_map/dot_general | solution.py:51
  21.9 46.7 %all-gather.7.cloned.1.call-done = bf16[2048,256]{1,0:T(8,128)(2,1)} async-done(((bf16[128,256]{1,0:T(8,128)(2,1)}), bf16[2048,256]{1,0:T(8,128)(2,1)}) %all-gather.7.cloned.1.call-update) | async-done | bytes 1048592 | tf_op jit(solution)/shard_map/all_gather | solution.py:45
  68.6 11.2 %convolution_bitcast_fusion.1 = f32[256,1024]{0,1:T(8,128)} fusion(f32[2048,1024]{1,0:T(8,128)} %fusion.4, bf16[2048,256]{1,0:T(8,128)(2,1)} %all-gather.7.cloned.1.call-done), kind=kOutput, calls=%fused_computation.2 | convolution fusion | flops 6442450944 | bytes 10485760 | tf_op jit(solution)/shard_map/dot_general | solution.py:56
  79.8 45.5 %all-gather.9.cloned.1.call-done = bf16[2048,256]{1,0:T(8,128)(2,1)} async-done(((bf16[128,256]{1,0:T(8,128)(2,1)}), bf16[2048,256]{1,0:T(8,128)(2,1)}) %all-gather.9.cloned.1.call-update) | async-done | bytes 1048592 | tf_op jit(solution)/shard_map/all_gather | solution.py:46
  125.3 9.5 %convolution_bitcast_fusion = f32[256,1024]{0,1:T(8,128)S(1)} fusion(f32[2048,1024]{1,0:T(8,128)} %fusion.5, bf16[2048,256]{1,0:T(8,128)(2,1)} %all-gather.9.cloned.1.call-done), kind=kOutput, calls=%fused_computation.1 | convolution fusion | flops 6442450944 | bytes 10485760 | tf_op jit(solution)/shard_map/dot_general | solution.py:57
  134.8 0.0 copy-done.1
  134.8 1.5 pad_maximum_fusion
  136.2 0.0 copy-start.2
  136.3 2.9 copy.65
  139.2 0.0 reduce-scatter.4.cloned.1.call-update
  139.2 0.0 all-gather.13.cloned.1.call-start
  139.3 80.4 %reduce-scatter.4.cloned.1.call-done = f32[16,2048]{1,0:T(8,128)} async-done(((f32[256,2048]{1,0:T(8,128)}), f32[16,2048]{1,0:T(8,128)}) %reduce-scatter.4.cloned.1.call-update) | async-done | bytes 131088 | tf_op jit(solution)/shard_map/reduce_scatter | solution.py:58
  219.7 0.0 copy-done.4
  219.7 0.0 copy-done.5
  219.7 1.6 add_divide_fusion
  221.3 0.0 all-gather.13.cloned.1.call-update
  221.3 0.0 all-gather.11.cloned.1.call-start
  221.4 0.5 all-gather.11.cloned.1.call-update
  221.9 0.0 all-gather.15.cloned.1.call-start
  222.0 2.0 copy.59
  224.0 50.6 %all-gather.13.cloned.1.call-done = f32[256,1024]{1,0:T(8,128)} async-done(((f32[16,1024]{1,0:T(8,128)}), f32[256,1024]{1,0:T(8,128)}) %all-gather.13.cloned.1.call-update) | async-done | bytes 1048592 | tf_op jit(solution)/shard_map/all_gather | solution.py:66
  274.6 0.0 copy-done.2
  274.6 3.6 multiply_reduce_fusion
  278.3 53.5 %all-gather.11.cloned.1.call-done = f32[256,1024]{1,0:T(8,128)} async-done(((f32[16,1024]{1,0:T(8,128)}), f32[256,1024]{1,0:T(8,128)}) %all-gather.11.cloned.1.call-update) | async-done | bytes 1048592 | tf_op jit(solution)/shard_map/all_gather | solution.py:65
  331.8 3.6 multiply_reduce_fusion.1
  335.4 40.3 %all-reduce = (f32[]{:T(128)}, f32[]{:T(128)}) all-reduce(f32[]{:T(128)} %get-tuple-element.49, f32[]{:T(128)} %get-tuple-element.51), channel_id=1, replica_groups=mesh['fs'=16,'tp'=2] {'fs'}, use_global_device_ids=true, to_apply=%region_2.0 | all-reduce | flops 2 | bytes 16 | tf_op jit(solution)/shard_map/psum | solution.py:16
  375.7 3.2 all-reduce.1
  379.5 2.2 subtract_convert_fusion.1
  381.7 0.0 all-gather.15.cloned.1.call-update
  381.7 0.0 all-gather.17.cloned.1.call-start
  381.7 2.0 copy.60
  384.5 2.2 subtract_convert_fusion
  386.7 0.0 all-gather.17.cloned.1.call-update
  386.8 2.1 copy.61
  388.8 2.0 copy.62
  390.8 75.6 %all-gather.15.cloned.1.call-done = bf16[2048,1024]{0,1:T(8,128)(2,1)} async-done(((bf16[128,1024]{0,1:T(8,128)(2,1)}), bf16[2048,1024]{0,1:T(8,128)(2,1)}) %all-gather.15.cloned.1.call-update) | async-done | bytes 4194320 | tf_op jit(solution)/shard_map/all_gather | solution.py:79
  466.5 6.4 %copy.63 = bf16[2048,1024]{1,0:T(8,128)(2,1)} copy(bf16[2048,1024]{0,1:T(8,128)(2,1)} %all-gather.15.cloned.1.call-done) | data formatting | bytes 8388608
  472.9 83.2 %all-gather.17.cloned.1.call-done = bf16[2048,1024]{0,1:T(8,128)(2,1)} async-done(((bf16[128,1024]{0,1:T(8,128)(2,1)}), bf16[2048,1024]{0,1:T(8,128)(2,1)}) %all-gather.17.cloned.1.call-update) | async-done | bytes 4194320 | tf_op jit(solution)/shard_map/all_gather | solution.py:80
  556.1 6.4 %copy.64 = bf16[2048,1024]{1,0:T(8,128)(2,1)} copy(bf16[2048,1024]{0,1:T(8,128)(2,1)} %all-gather.17.cloned.1.call-done) | data formatting | bytes 8388608
  (10 shorter events, 0.0 us)
Async XLA Ops:
  7.2 1.9 copy-start
  7.2 61.4 %all-gather.7.cloned.1.call-start = ((), (), s32[]{:S(2)}) async-start(), calls=%async_computation.1 | async-start | bytes 1114112 | tf_op jit(solution)/shard_map/all_gather | solution.py:45
  7.9 117.4 %all-gather.9.cloned.1.call-start = ((), (), s32[]{:S(2)}) async-start(), calls=%async_computation.2 | async-start | bytes 1114112 | tf_op jit(solution)/shard_map/all_gather | solution.py:46
  8.7 211.0 %reduce-scatter.4.cloned.1.call-start = ((), (), s32[]{:S(2)}) async-start(), calls=%async_computation.7 | async-start | bytes 2228224 | tf_op jit(solution)/shard_map/reduce_scatter | solution.py:58
  9.1 7.2 %copy-start.8 = (bf16[768,1024]{1,0:T(8,128)(2,1)S(1)}, bf16[768,1024]{1,0:T(8,128)(2,1)}, u32[]{:S(2)}) copy-start(bf16[768,1024]{1,0:T(8,128)(2,1)} %param.13) | copy-start | bytes 4718596
  125.3 9.5 %copy-start.1 = (f32[256,1024]{0,1:T(8,128)S(1)}, f32[256,1024]{0,1:T(8,128)}, u32[]{:S(2)}) copy-start(f32[256,1024]{0,1:T(8,128)} %convolution_bitcast_fusion.1) | copy-start | bytes 3145732
  136.2 83.4 %copy-start.4 = (f32[16,1024]{1,0:T(8,128)S(1)}, f32[16,1024]{1,0:T(8,128)}, u32[]{:S(2)}) copy-start(f32[16,1024]{1,0:T(8,128)} %param.21) | copy-start | bytes 196612
  136.2 83.4 %copy-start.5 = (f32[16,1024]{1,0:T(8,128)S(1)}, f32[16,1024]{1,0:T(8,128)}, u32[]{:S(2)}) copy-start(f32[16,1024]{1,0:T(8,128)} %param.20) | copy-start | bytes 196612
  136.2 83.4 %copy-start.6 = (f32[16,1024]{1,0:T(8,128)S(1)}, f32[16,1024]{1,0:T(8,128)}, u32[]{:S(2)}) copy-start(f32[16,1024]{1,0:T(8,128)} %param.19) | copy-start | bytes 196612
  136.2 83.4 %copy-start.7 = (f32[16,1024]{1,0:T(8,128)S(1)}, f32[16,1024]{1,0:T(8,128)}, u32[]{:S(2)}) copy-start(f32[16,1024]{1,0:T(8,128)} %param.18) | copy-start | bytes 196612
  136.2 138.4 %copy-start.2 = (bf16[128,256]{1,0:T(8,128)(2,1)S(1)}, bf16[128,256]{1,0:T(8,128)(2,1)}, u32[]{:S(2)}) copy-start(bf16[128,256]{1,0:T(8,128)(2,1)} %param.17) | copy-start | bytes 196612
  139.2 192.6 %copy-start.3 = (bf16[128,256]{1,0:T(8,128)(2,1)S(1)}, bf16[128,256]{1,0:T(8,128)(2,1)}, u32[]{:S(2)}) copy-start(bf16[128,256]{1,0:T(8,128)(2,1)} %param.16) | copy-start | bytes 196612
  139.2 135.4 %all-gather.13.cloned.1.call-start = ((), (), s32[]{:S(2)}) async-start(), calls=%async_computation.4 | async-start | bytes 1114112 | tf_op jit(solution)/shard_map/all_gather | solution.py:66
  221.3 110.4 %all-gather.11.cloned.1.call-start = ((), (), s32[]{:S(2)}) async-start(), calls=%async_computation.3 | async-start | bytes 1114112 | tf_op jit(solution)/shard_map/all_gather | solution.py:65
  221.9 244.6 %all-gather.15.cloned.1.call-start = ((), (), s32[]{:S(2)}) async-start(), calls=%async_computation.5 | async-start | bytes 4456448 | tf_op jit(solution)/shard_map/all_gather | solution.py:79
  381.7 174.4 %all-gather.17.cloned.1.call-start = ((), (), s32[]{:S(2)}) async-start(), calls=%async_computation.6 | async-start | bytes 4456448 | tf_op jit(solution)/shard_map/all_gather | solution.py:80
Sparse Core Ops, SparseCore 0:
  10.7 57.7 all-gather.6
  71.3 53.9 all-gather.8
  139.3 80.2 reduce-scatter.3
  222.9 51.7 all-gather.12
  277.8 53.9 all-gather.10
  381.8 84.6 all-gather.14
  469.2 86.8 all-gather.16
